TPU v7x, 32 devices: a whole 2x2x4 slice. The times are simulated.
32 devices in a mesh: ep: 16 (over z, x, core), tp: 2 (over y).
Axes of the slice: x: 2, y: 2, z: 4, core: 2. Of those that a mesh axis runs over, the one named last changes fastest.
Arguments:
- tokens: bfloat16 [256, 1024], P('ep'), may hold values from -6 to 6
- state: float32 [256, 16, 64, 64], P('ep', 'tp'), may hold values from -6 to 6
- w_recep: bfloat16 [1024, 1024], P(None, 'tp'), may hold values from -0.1875 to 0.1875
- w_key: bfloat16 [1024, 1024], P(None, 'tp'), may hold values from -0.1875 to 0.1875
- w_value: bfloat16 [1024, 1024], P(None, 'tp'), may hold values from -0.1875 to 0.1875
- w_out: bfloat16 [1024, 1024], P('tp'), may hold values from -0.1875 to 0.1875
- decay_base: float32 [1024], P('tp'), may hold values from -5 to 1
- decay_down: bfloat16 [1024, 64], replicated, may hold values from -0.1875 to 0.1875
- decay_up: bfloat16 [64, 1024], P(None, 'tp'), may hold values from -1 to 1
- rate_base: float32 [1024], P('tp'), may hold values from -4 to 4
- rate_down: bfloat16 [1024, 64], replicated, may hold values from -0.1875 to 0.1875
- rate_up: bfloat16 [64, 1024], P(None, 'tp'), may hold values from -1 to 1
- head_gain: float32 [1024], P('tp'), may hold values from 0.1 to 1.9
- first_gain: float32 [1024], replicated, may hold values from 0.2 to 4.8
- expert_gate: bfloat16 [16, 1024, 1408], P('ep', None, 'tp'), may hold values from -0.1875 to 0.1875
- expert_up: bfloat16 [16, 1024, 1408], P('ep', None, 'tp'), may hold values from -0.1875 to 0.1875
- expert_down: bfloat16 [16, 1408, 1024], P('ep', 'tp'), may hold values from -0.078125 to 0.078125
- dense_gate: bfloat16 [2816, 1024], P('ep'), may hold values from -0.1875 to 0.1875
- dense_up: bfloat16 [2816, 1024], P('ep'), may hold values from -0.1875 to 0.1875
- dense_down: bfloat16 [2816, 1024], P('ep', 'tp'), may hold values from -0.21875 to 0.21875
- branch_gate: bfloat16 [1024], replicated, may hold values from -0.1875 to 0.1875
- second_gain: float32 [1024], P('tp'), may hold values from 0.1 to 1.9
- routes: int32 [256, 2], P('ep'), may hold values from 0 to 3, all different within a row; in each aligned block of 16 rows (0 to 15, 16 to 31, ...) at most 16 rows name the same one
- route_weights: float32 [256, 2], P('ep'), may hold values from 0.2 to 1
Outputs:
- layer_output: bfloat16 [256, 1024], P('ep', 'tp')
Inputs may be any that keep to these rules, and one draw needn't show every extreme that they name: `routes`: each row names 2 different experts. In each aligned block of 16 rows no expert is named by more than 16 rows, a bound that some block reaches.
All inputs are finite; a program needn't handle non-finite values.
Results may differ from a plain program's by a relative error of at most 0.018.
Values may be sent and summed in bfloat16 or wider, within the bound.
A program may use at most 64 MiB of HBM per device.

v0:
```python
import jax
import jax.numpy as jnp
from jax import lax
from jax.sharding import PartitionSpec as P

SPLIT = 4
residual_scale = 1.4142135623730951
norm_epsilon = 1e-05
head_epsilon = 0.00064
key_epsilon = 1e-06


def time_mixer(
    tokens,
    state,
    w_recep,
    w_key,
    w_value,
    w_out,
    decay_base,
    decay_down,
    decay_up,
    rate_base,
    rate_down,
    rate_up,
    head_gain,
):
    row_count = tokens.shape[0]
    head_count = state.shape[1]
    head_size = state.shape[3]
    recep = jnp.dot(tokens, w_recep, preferred_element_type=jnp.float32).reshape(
        row_count, head_count, head_size
    )
    key_vecs = jnp.dot(tokens, w_key, preferred_element_type=jnp.float32).reshape(
        row_count, head_count, head_size
    )
    value_vecs = jnp.dot(tokens, w_value, preferred_element_type=jnp.float32).reshape(
        row_count, head_count, head_size
    )
    decay_low = jnp.tanh(jnp.dot(tokens, decay_down, preferred_element_type=jnp.float32)).astype(
        jnp.bfloat16
    )
    decay_pre = decay_base + jnp.dot(decay_low, decay_up, preferred_element_type=jnp.float32)
    log_rate = -jax.nn.softplus(-decay_pre) - 0.5
    decay = jnp.exp(-jnp.exp(log_rate)).reshape(row_count, head_count, head_size)
    rate_low = jnp.dot(tokens, rate_down, preferred_element_type=jnp.float32).astype(jnp.bfloat16)
    in_rate = jax.nn.sigmoid(
        rate_base + jnp.dot(rate_low, rate_up, preferred_element_type=jnp.float32)
    ).reshape(row_count, head_count, head_size)
    unit_keys = key_vecs * lax.rsqrt(jnp.sum(key_vecs * key_vecs, -1, keepdims=True) + key_epsilon)
    removed = jnp.einsum("bhij,bhj->bhi", state, -unit_keys)
    updated = (
        state * decay[:, :, None, :]
        + removed[..., None] * (unit_keys * in_rate)[:, :, None, :]
        + value_vecs[..., None] * key_vecs[:, :, None, :]
    )
    read_out = jnp.einsum("bhij,bhj->bhi", updated, recep)
    centre = jnp.mean(read_out, -1, keepdims=True)
    spread = jnp.mean(jnp.square(read_out - centre), -1, keepdims=True)
    normed = ((read_out - centre) * lax.rsqrt(spread + head_epsilon)).reshape(
        row_count, head_count * head_size
    ) * head_gain
    return jnp.dot(normed.astype(jnp.bfloat16), w_out, preferred_element_type=jnp.float32)


def first_norm(values, gain):
    centre = jnp.mean(values, -1, keepdims=True)
    spread = jnp.mean(jnp.square(values - centre), -1, keepdims=True)
    return ((values - centre) * lax.rsqrt(spread + norm_epsilon) * gain).astype(jnp.bfloat16)


def route_tables(routes, route_weights, experts, capacity):
    expert_hits = (
        routes[:, :, None] == jnp.arange(experts, dtype=jnp.int32)[None, None, :]
    ).astype(jnp.int32)
    row_hits = jnp.sum(expert_hits, 1, dtype=jnp.int32)
    earlier = jnp.cumsum(row_hits, 0, dtype=jnp.int32) - row_hits
    slot_index = jnp.sum(earlier[:, None, :] * expert_hits, 2, dtype=jnp.int32)
    target = routes * capacity + slot_index
    places = jnp.arange(experts * capacity, dtype=jnp.int32)
    slot_match = target[:, :, None] == places[None, None, :]
    dispatch_tokens = jnp.any(slot_match, 1).astype(jnp.bfloat16)
    combine_experts = jnp.sum(jnp.where(slot_match, route_weights[:, :, None], 0.0), 1)
    return (dispatch_tokens, combine_experts)


def shards(
    tokens,
    state,
    w_recep,
    w_key,
    w_value,
    w_out,
    decay_base,
    decay_down,
    decay_up,
    rate_base,
    rate_down,
    rate_up,
    head_gain,
    first_gain,
    expert_gate,
    expert_up,
    expert_down,
    dense_gate,
    dense_up,
    dense_down,
    branch_gate,
    second_gain,
    routes,
    route_weights,
):
    row_count = tokens.shape[0]
    model_width = tokens.shape[1]
    quarter = w_recep.shape[1]
    tp_index = lax.axis_index("tp")
    partial_mix = time_mixer(
        tokens,
        state,
        w_recep,
        w_key,
        w_value,
        w_out,
        decay_base,
        decay_down,
        decay_up,
        rate_base,
        rate_down,
        rate_up,
        head_gain,
    )
    mixed = lax.psum(partial_mix, "tp")
    x_mid = first_norm(residual_scale * tokens.astype(jnp.float32) + mixed, first_gain)
    own_columns = lax.dynamic_slice_in_dim(x_mid, tp_index * quarter, quarter, 1)
    experts = lax.axis_size("ep") // SPLIT
    capacity = min(row_count, max(2, 2 * row_count * routes.shape[1] // experts))
    dispatch_tokens, combine_experts = route_tables(routes, route_weights, experts, capacity)
    packed_rows = lax.dot_general(
        dispatch_tokens, x_mid, (((0,), (0,)), ((), ())), preferred_element_type=jnp.float32
    ).astype(jnp.bfloat16)
    outgoing = jnp.repeat(packed_rows.reshape(experts, capacity, x_mid.shape[1]), SPLIT, axis=0)
    arrived = lax.all_to_all(outgoing, "ep", split_axis=0, concat_axis=0, tiled=True)
    sources = arrived.shape[0]
    slot_count = arrived.shape[1]
    flat_rows = arrived.reshape(sources * slot_count, model_width)
    gate_pre = jnp.dot(flat_rows, expert_gate[0], preferred_element_type=jnp.float32)
    up_pre = jnp.dot(flat_rows, expert_up[0], preferred_element_type=jnp.float32)
    hidden = (jax.nn.silu(gate_pre) * up_pre).astype(jnp.bfloat16)
    partial_out = jnp.dot(hidden, expert_down[0], preferred_element_type=jnp.float32).reshape(
        sources, slot_count, model_width
    )
    summed = lax.psum_scatter(
        partial_out.astype(jnp.bfloat16), "tp", scatter_dimension=2, tiled=True
    ).astype(jnp.float32)
    returned = lax.all_to_all(
        summed.astype(jnp.bfloat16), "ep", split_axis=0, concat_axis=0, tiled=True
    ).astype(summed.dtype)
    expert_out = jnp.sum(returned.reshape(experts, SPLIT, capacity, quarter), 1).reshape(
        experts * capacity, quarter
    )
    routed_part = jnp.dot(
        combine_experts,
        expert_out,
        precision=lax.Precision.HIGHEST,
        preferred_element_type=jnp.float32,
    )
    branch = jax.nn.sigmoid(jnp.dot(x_mid, branch_gate, preferred_element_type=jnp.float32))
    shard_rows = lax.all_gather(x_mid, "ep", axis=0, tiled=True)
    gate_pre = lax.dot_general(
        shard_rows, dense_gate, (((1,), (1,)), ((), ())), preferred_element_type=jnp.float32
    )
    up_pre = lax.dot_general(
        shard_rows, dense_up, (((1,), (1,)), ((), ())), preferred_element_type=jnp.float32
    )
    dense_hidden = (jax.nn.silu(gate_pre) * up_pre).astype(jnp.bfloat16)
    dense_part = lax.psum_scatter(
        jnp.dot(dense_hidden, dense_down, preferred_element_type=jnp.float32),
        "ep",
        scatter_dimension=0,
        tiled=True,
    )
    second_sum = (
        residual_scale * own_columns.astype(jnp.float32)
        + routed_part
        + branch[:, None] * dense_part
    )
    row_sums, square_sums = lax.psum(
        (jnp.sum(second_sum, 1), jnp.sum(second_sum * second_sum, 1)), "tp"
    )
    average = row_sums / model_width
    spread = square_sums / model_width - average * average
    return (
        (second_sum - average[:, None]) * lax.rsqrt(spread + norm_epsilon)[:, None] * second_gain
    ).astype(jnp.bfloat16)


def solution(mesh):
    return jax.shard_map(
        shards,
        mesh=mesh,
        in_specs=(
            P("ep", None),
            P("ep", "tp", None, None),
            P(None, "tp"),
            P(None, "tp"),
            P(None, "tp"),
            P("tp", None),
            P("tp"),
            P(),
            P(None, "tp"),
            P("tp"),
            P(),
            P(None, "tp"),
            P("tp"),
            P(),
            P("ep", None, "tp"),
            P("ep", None, "tp"),
            P("ep", "tp", None),
            P("ep", None),
            P("ep", None),
            P("ep", "tp"),
            P(),
            P("tp"),
            P("ep", None),
            P("ep", None),
        ),
        out_specs=P("ep", "tp"),
        check_vma=False,
    )
```

profile of v0, /device:TPU:0, one launch (start us, length us, event | category | flops | bytes accessed | tf_op | source)
XLA Modules:
  0.0 162.2 jit_solution(11377209794120408051)
XLA Ops:
  6.5 1.6 fusion.56
  8.3 1.2 fusion.32
  9.6 1.5 fusion.59
  11.2 1.3 fusion.49
  12.6 1.5 fusion.58
  14.2 3.5 %fusion.57 = f32[16,8,1,64]{3,2,1,0:T(1,128)S(1)} fusion(f32[16,8,64,1]{2,3,1,0:T(1,128)S(1)} %bitcast.81, f32[16,8,64,64]{3,2,1,0:T(8,128)} %param.25), kind=kOutput, calls=%fused_computation.85 | convolution fusion | flops 1048576 | bytes 2162688 | tf_op jit(solution)/shard_map/bhij,bhj->bhi/dot_general | solution.py:51
  17.8 2.9 %fusion = f32[16,8,1,64]{3,2,1,0:T(1,128)S(1)} fusion(f32[16,8,64,1]{2,3,1,0:T(1,128)S(1)} %bitcast.83, f32[16,8,64,64]{3,2,1,0:T(8,128)S(1)} %copy-done.1, f32[16,8,64]{2,1,0:T(8,128)S(1)} %reshape.96, f32[16,8,64]{2,1,0:T(8,128)S(1)} %mul.177, f32[16,8,64]{2,1,0:T(8,128)S(1)} %get-tuple-element.10, f32[16,8,64]{2,1,0:T(8,128)S(1)} %bitcast.82, ...), kind=kOutput, calls=%fused_computation | convolution fusion | flops 3670016 | bytes 2326528 | tf_op jit(solution)/shard_map/bhij,bhj->bhi/dot_general | solution.py:57
  21.2 2.1 %fusion.51 = f32[16,1024]{1,0:T(8,128)} fusion(bf16[512,1024]{1,0:T(8,128)(2,1)} %param.29, f32[16,512]{1,0:T(8,128)S(1)} %reshape.99, f32[512]{0:T(512)S(1)} %copy-done.7), kind=kOutput, calls=%fused_computation.66 | convolution fusion | flops 16793600 | bytes 1148928 | tf_op jit(solution)/shard_map/dot_general | solution.py:63
  23.7 23.4 %all-reduce.3.cloned.1.call-done = f32[16,1024]{1,0:T(8,128)} async-done(((f32[16,1024]{1,0:T(8,128)}), f32[16,1024]{1,0:T(8,128)}) %all-reduce.3.cloned.1.call-update) | async-done | bytes 65552 | tf_op jit(solution)/shard_map/psum | solution.py:132
  47.2 1.1 fusion.50
  48.2 1.0 multiply_reduce_fusion
  49.3 0.9 multiply_convert_fusion
  50.5 19.7 %all_to_all.10 = bf16[16,16,1024]{2,1,0:T(8,128)(2,1)S(1)} all-to-all(bf16[16,16,1024]{2,1,0:T(8,128)(2,1)S(1)} %bitcast.72), channel_id=1, replica_groups=mesh['ep'=16,'tp'=2] {'ep'}, dimensions={0} | all-to-all | bytes 1048576 | tf_op jit(solution)/shard_map/all_to_all | solution.py:142
  70.2 0.6 fusion.15
  70.8 0.6 fusion.23
  71.6 1.4 fusion.17
  73.1 21.3 %all_gather.3 = bf16[256,1024]{1,0:T(8,128)(2,1)S(1)} all-gather(bf16[16,1024]{1,0:T(8,128)(2,1)S(1)} %multiply_convert_fusion), channel_id=1, replica_groups=mesh['ep'=16,'tp'=2] {'ep'}, dimensions={0}, use_global_device_ids=true | all-gather | bytes 557056 | tf_op jit(solution)/shard_map/all_gather | solution.py:168
  94.8 1.5 fusion.27
  96.3 3.5 %all-to-all-start.1 = ((bf16[16,16,512]{2,1,0:T(8,128)(2,1)}), bf16[16,16,512]{2,1,0:T(8,128)(2,1)S(1)}, u32[]{:S(2)}, u32[]{:S(2)}) async-start(bf16[16,16,512]{2,1,0:T(8,128)(2,1)} %reduce-scatter.3.cloned.1.call-done), calls=%async_computation.2 | async-start | bytes 524288 | tf_op jit(solution)/shard_map/all_to_all | solution.py:155
  100.1 9.7 %all-to-all-done.1 = bf16[16,16,512]{2,1,0:T(8,128)(2,1)S(1)} async-done(((bf16[16,16,512]{2,1,0:T(8,128)(2,1)}), bf16[16,16,512]{2,1,0:T(8,128)(2,1)S(1)}, u32[]{:S(2)}, u32[]{:S(2)}) %all-to-all-start.1) | async-done | bytes 262176 | tf_op jit(solution)/shard_map/all_to_all | solution.py:155
  109.9 39.1 %reduce-scatter.5.cloned.1.call-done = f32[16,512]{1,0:T(8,128)} async-done(((f32[256,512]{1,0:T(8,128)}), f32[16,512]{1,0:T(8,128)}) %reduce-scatter.5.cloned.1.call-update) | async-done | bytes 32784 | tf_op jit(solution)/shard_map/reduce_scatter | solution.py:176
  148.9 1.1 fusion.55
  150.0 4.9 %all-reduce = (f32[16]{0:T(128)S(1)}, f32[16]{0:T(128)S(1)}) all-reduce(f32[16]{0:T(128)S(1)} %get-tuple-element.6, f32[16]{0:T(128)S(1)} %get-tuple-element.5), channel_id=1, replica_groups=mesh['ep'=16,'tp'=2] {'tp'}, use_global_device_ids=true, to_apply=%region_17.18 | all-reduce | flops 32 | bytes 256 | tf_op jit(solution)/shard_map/psum | solution.py:187
  154.9 0.7 multiply_convert_fusion.1
  (68 shorter events, 2.7 us)
Async XLA Ops:
  6.5 65.1 %copy-start = (bf16[1,704,1024]{2,1,0:T(8,128)(2,1)S(1)}, bf16[1,704,1024]{2,1,0:T(8,128)(2,1)}, u32[]{:S(2)}) copy-start(bf16[1,704,1024]{2,1,0:T(8,128)(2,1)} %param.40) | copy-start | bytes 4325380
  6.5 40.6 %all-reduce.3.cloned.1.call-start = ((), (), s32[]{:S(2)}) async-start(), calls=%async_computation.4 | async-start | bytes 131072 | tf_op jit(solution)/shard_map/psum | solution.py:132
  14.1 3.6 %copy-start.1 = (f32[16,8,64,64]{3,2,1,0:T(8,128)S(1)}, f32[16,8,64,64]{3,2,1,0:T(8,128)}, u32[]{:S(2)}) copy-start(f32[16,8,64,64]{3,2,1,0:T(8,128)} %param.25) | copy-start | bytes 6291460
  17.7 3.5 %copy-start.7 = (f32[512]{0:T(512)S(1)}, f32[512]{0:T(512)}, u32[]{:S(2)}) copy-start(f32[512]{0:T(512)} %param.36) | copy-start | bytes 6148
  17.7 5.6 %copy-start.5 = (s32[16,2]{0,1:T(2,128)S(1)}, s32[16,2]{0,1:T(2,128)}, u32[]{:S(2)}) copy-start(s32[16,2]{0,1:T(2,128)} %param.46) | copy-start | bytes 388
  17.7 29.4 %copy-start.2 = (bf16[16,1024]{1,0:T(8,128)(2,1)S(1)}, bf16[16,1024]{1,0:T(8,128)(2,1)}, u32[]{:S(2)}) copy-start(bf16[16,1024]{1,0:T(8,128)(2,1)} %param.24) | copy-start | bytes 98308
  17.8 31.5 %copy-start.6 = (f32[1024]{0:T(1024)S(1)}, f32[1024]{0:T(1024)}, u32[]{:S(2)}) copy-start(f32[1024]{0:T(1024)} %param.37) | copy-start | bytes 12292
  17.8 52.4 %copy-start.3 = (bf16[1,1024,704]{1,2,0:T(8,128)(2,1)S(1)}, bf16[1,1024,704]{1,2,0:T(8,128)(2,1)}, u32[]{:S(2)}) copy-start(bf16[1,1024,704]{1,2,0:T(8,128)(2,1)} %param.38) | copy-start | bytes 4325380
  23.3 73.0 %reduce-scatter.3.cloned.1.call-start = ((), (), s32[]{:S(2)}) async-start(), calls=%async_computation.5 | async-start | bytes 786432 | tf_op jit(solution)/shard_map/reduce_scatter | solution.py:152
  47.2 23.6 %copy-start.11 = (bf16[1,1024,704]{1,2,0:T(8,128)(2,1)S(1)}, bf16[1,1024,704]{1,2,0:T(8,128)(2,1)}, u32[]{:S(2)}) copy-start(bf16[1,1024,704]{1,2,0:T(8,128)(2,1)} %param.39) | copy-start | bytes 4325380
  70.8 23.6 %copy-start.4 = (bf16[176,1024]{1,0:T(8,128)(2,1)S(1)}, bf16[176,1024]{1,0:T(8,128)(2,1)}, u32[]{:S(2)}) copy-start(bf16[176,1024]{1,0:T(8,128)(2,1)} %param.41) | copy-start | bytes 1081348
  70.8 23.9 %copy-start.12 = (bf16[176,1024]{1,0:T(8,128)(2,1)S(1)}, bf16[176,1024]{1,0:T(8,128)(2,1)}, u32[]{:S(2)}) copy-start(bf16[176,1024]{1,0:T(8,128)(2,1)} %param.42) | copy-start | bytes 1081348
  70.8 23.9 %copy-start.13 = (bf16[176,512]{1,0:T(8,128)(2,1)S(1)}, bf16[176,512]{1,0:T(8,128)(2,1)}, u32[]{:S(2)}) copy-start(bf16[176,512]{1,0:T(8,128)(2,1)} %param.43) | copy-start | bytes 540676
  71.4 28.4 %copy-start.8 = (bf16[1024]{0:T(1024)(128)(2,1)S(1)}, bf16[1024]{0:T(1024)(128)(2,1)}, u32[]{:S(2)}) copy-start(bf16[1024]{0:T(1024)(128)(2,1)} %param.44) | copy-start | bytes 6148
  71.4 28.4 %copy-start.10 = (f32[16,2]{0,1:T(2,128)S(1)}, f32[16,2]{0,1:T(2,128)}, u32[]{:S(2)}) copy-start(f32[16,2]{0,1:T(2,128)} %param.47) | copy-start | bytes 388
  71.6 83.3 %copy-start.9 = (f32[512]{0:T(512)S(1)}, f32[512]{0:T(512)}, u32[]{:S(2)}) copy-start(f32[512]{0:T(512)} %param.45) | copy-start | bytes 6148
  73.1 75.9 %reduce-scatter.5.cloned.1.call-start = ((), (), s32[]{:S(2)}) async-start(), calls=%async_computation.6 | async-start | bytes 557056 | tf_op jit(solution)/shard_map/reduce_scatter | solution.py:176
  96.3 13.5 %all-to-all-start.1 = ((bf16[16,16,512]{2,1,0:T(8,128)(2,1)}), bf16[16,16,512]{2,1,0:T(8,128)(2,1)S(1)}, u32[]{:S(2)}, u32[]{:S(2)}) async-start(bf16[16,16,512]{2,1,0:T(8,128)(2,1)} %reduce-scatter.3.cloned.1.call-done), calls=%async_computation.2 | async-start | bytes 524288 | tf_op jit(solution)/shard_map/all_to_all | solution.py:155
Sparse Core Ops, SparseCore 0:
  23.4 23.6 all-reduce.2
  73.2 13.2 reduce-scatter.2
  96.4 52.5 reduce-scatter.4
where the time goes:
time: 163 us; the launch traced here: 162 us
  waiting for transfers between devices  72.3 us (44%)
  blocking collectives  45.9 us (28%)
  matrix products  21.3 us (13%)
  between operations  13.4 us (8%)
  other arithmetic  4.56 us (3%)
  starting transfers between devices  3.63 us (2%)
    reduce_scatter x1, waiting for transfers between devices, shards(): lax.psum_scatter(jnp.dot(dense_hidden, dense_down, preferred_element_type...  39.1 us
    psum x1, waiting for transfers between devices, shards(): mixed = lax.psum(partial_mix, 'tp')  23.4 us
    all_gather x1, blocking collectives, shards(): shard_rows = lax.all_gather(x_mid, 'ep', axis=0, tiled=True)  21.3 us
    all_to_all x1, blocking collectives, shards(): lax.all_to_all(outgoing, 'ep', split_axis=0, concat_axis=0, tiled=True)  19.7 us
    all_to_all x1, waiting for transfers between devices, shards(): lax.all_to_all(summed.astype(jnp.bfloat16), 'ep', split_axis=0, concat_ax...  9.73 us
    psum x1, blocking collectives, shards(): lax.psum((jnp.sum(second_sum, 1), jnp.sum(second_sum * second_sum, 1)), '...  4.93 us
    all_to_all x1, starting transfers between devices, shards(): lax.all_to_all(summed.astype(jnp.bfloat16), 'ep', split_axis=0, concat_ax...  3.54 us
    dot_general x1, matrix products, time_mixer(): removed = jnp.einsum('bhij,bhj->bhi', state, -unit_keys)  3.51 us
  transfers between devices with their start and end apart: 4, of which 3 were waited for; matrix products, arithmetic and copies ran while one was open for 1% of the time, Pallas kernels for 0%

commit v1 on v0

--- a/solution.py
+++ b/solution.py
@@ -129,7 +129,7 @@
         rate_up,
         head_gain,
     )
-    mixed = lax.psum(partial_mix, "tp")
+    mixed = jnp.sum(lax.all_gather(partial_mix, "tp"), axis=0)
     x_mid = first_norm(residual_scale * tokens.astype(jnp.float32) + mixed, first_gain)
     own_columns = lax.dynamic_slice_in_dim(x_mid, tp_index * quarter, quarter, 1)
     experts = lax.axis_size("ep") // SPLIT

time: 163 us -> 144 us (0.88)
  waiting for transfers between devices: 72.3 us -> 49.8 us
  blocking collectives: 45.9 us -> 52.6 us
  other arithmetic: 4.56 us -> 1.94 us
    psum x1 -> x0, waiting for transfers between devices: 23.4 us -> none  [shards(): mixed = lax.psum(partial_mix, 'tp')]
    all_gather x0 -> x1, blocking collectives: none -> 5.88 us  [shards(): mixed = jnp.sum(lax.all_gather(partial_mix, 'tp'), axis=0)]
  transfers between devices with their start and end apart: 4 -> 3, of which waited for: 3 -> 2; matrix products, arithmetic and copies ran while one was open for 1% -> 1% of each run, Pallas kernels for 0% -> 0%
where the time goes in v1:
time: 144 us; the launch traced here: 143 us
  blocking collectives  52.6 us (37%)
  waiting for transfers between devices  49.8 us (35%)
  matrix products  20.7 us (14%)
  between operations  13.7 us (10%)
  starting transfers between devices  3.59 us (2%)
  other arithmetic  1.94 us (1%)
    reduce_scatter x1, waiting for transfers between devices, shards(): lax.psum_scatter(jnp.dot(dense_hidden, dense_down, preferred_element_type...  40.1 us
    all_gather x1, blocking collectives, shards(): shard_rows = lax.all_gather(x_mid, 'ep', axis=0, tiled=True)  21.3 us
    all_to_all x1, blocking collectives, shards(): lax.all_to_all(outgoing, 'ep', split_axis=0, concat_axis=0, tiled=True)  20.5 us
    all_to_all x1, waiting for transfers between devices, shards(): lax.all_to_all(summed.astype(jnp.bfloat16), 'ep', split_axis=0, concat_ax...  9.73 us
    all_gather x1, blocking collectives, shards(): mixed = jnp.sum(lax.all_gather(partial_mix, 'tp'), axis=0)  5.88 us
    psum x1, blocking collectives, shards(): lax.psum((jnp.sum(second_sum, 1), jnp.sum(second_sum * second_sum, 1)), '...  4.93 us
    all_to_all x1, starting transfers between devices, shards(): lax.all_to_all(summed.astype(jnp.bfloat16), 'ep', split_axis=0, concat_ax...  3.55 us
    dot_general x1, matrix products, time_mixer(): removed = jnp.einsum('bhij,bhj->bhi', state, -unit_keys)  3.51 us
  transfers between devices with their start and end apart: 3, of which 2 were waited for; matrix products, arithmetic and copies ran while one was open for 1% of the time, Pallas kernels for 0%

profile of v1, /device:TPU:0, one launch (start us, length us, event | category | flops | bytes accessed | tf_op | source)
XLA Modules:
  0.0 143.4 jit_solution(1426825693756930415)
XLA Ops:
  6.5 1.6 %fusion.56 = f32[16,512]{1,0:T(8,128)S(1)} fusion(bf16[16,1024]{1,0:T(8,128)(2,1)} %param.24, bf16[1024,512]{1,0:T(8,128)(2,1)} %param.27), kind=kOutput, calls=%fused_computation.84 | convolution fusion | flops 16777216 | bytes 1114112 | tf_op jit(solution)/shard_map/dot_general | solution.py:34
  8.3 1.2 fusion.32
  9.6 1.5 %fusion.59 = f32[16,512]{1,0:T(8,128)S(1)} fusion(bf16[16,1024]{1,0:T(8,128)(2,1)} %param.24, bf16[1024,512]{1,0:T(8,128)(2,1)} %param.26), kind=kOutput, calls=%fused_computation.87 | convolution fusion | flops 16777216 | bytes 1114112 | tf_op jit(solution)/shard_map/dot_general | solution.py:31
  11.2 1.3 fusion.49
  12.6 1.5 %fusion.58 = f32[16,512]{1,0:T(8,128)S(1)} fusion(bf16[16,1024]{1,0:T(8,128)(2,1)} %param.24, bf16[1024,512]{1,0:T(8,128)(2,1)} %param.28), kind=kOutput, calls=%fused_computation.86 | convolution fusion | flops 16777216 | bytes 1114112 | tf_op jit(solution)/shard_map/dot_general | solution.py:37
  14.2 3.5 %fusion.57 = f32[16,8,1,64]{3,2,1,0:T(1,128)S(1)} fusion(f32[16,8,64,1]{2,3,1,0:T(1,128)S(1)} %bitcast.83, f32[16,8,64,64]{3,2,1,0:T(8,128)} %param.25), kind=kOutput, calls=%fused_computation.85 | convolution fusion | flops 1048576 | bytes 2162688 | tf_op jit(solution)/shard_map/bhij,bhj->bhi/dot_general | solution.py:51
  17.8 2.9 %fusion = f32[16,8,1,64]{3,2,1,0:T(1,128)S(1)} fusion(f32[16,8,64,1]{2,3,1,0:T(1,128)S(1)} %bitcast.85, f32[16,8,64,64]{3,2,1,0:T(8,128)S(1)} %copy-done.1, f32[16,8,64]{2,1,0:T(8,128)S(1)} %reshape.96, f32[16,8,64]{2,1,0:T(8,128)S(1)} %mul.177, f32[16,8,64]{2,1,0:T(8,128)S(1)} %get-tuple-element.10, f32[16,8,64]{2,1,0:T(8,128)S(1)} %bitcast.84, ...), kind=kOutput, calls=%fused_computation | convolution fusion | flops 3670016 | bytes 2326528 | tf_op jit(solution)/shard_map/bhij,bhj->bhi/dot_general | solution.py:57
  21.2 1.5 %fusion.51 = f32[16,1024]{1,0:T(8,128)S(1)} fusion(bf16[512,1024]{1,0:T(8,128)(2,1)} %param.29, f32[16,512]{1,0:T(8,128)S(1)} %reshape.99, f32[512]{0:T(512)S(1)} %copy-done.7), kind=kOutput, calls=%fused_computation.66 | convolution fusion | flops 16793600 | bytes 1148928 | tf_op jit(solution)/shard_map/dot_general | solution.py:63
  22.7 5.9 %all-gather = f32[32,1024]{1,0:T(8,128)S(1)} all-gather(f32[16,1024]{1,0:T(8,128)S(1)} %fusion.51), channel_id=2, replica_groups=mesh['ep'=16,'tp'=2] {'tp'}, dimensions={0}, use_global_device_ids=true | all-gather | bytes 196608 | tf_op jit(solution)/shard_map/all_gather | solution.py:132
  28.7 0.2 multiply_reduce_fusion
  29.4 0.2 convolution_convert_fusion
  29.7 20.5 %all_to_all.10 = bf16[16,16,1024]{2,1,0:T(8,128)(2,1)S(1)} all-to-all(bf16[16,16,1024]{2,1,0:T(8,128)(2,1)S(1)} %bitcast.73), channel_id=1, replica_groups=mesh['ep'=16,'tp'=2] {'ep'}, dimensions={0} | all-to-all | bytes 1048576 | tf_op jit(solution)/shard_map/all_to_all | solution.py:142
  50.2 0.6 fusion.15
  50.8 0.6 fusion.23
  51.6 1.4 fusion.17
  53.1 21.3 %all_gather.11 = bf16[256,1024]{1,0:T(8,128)(2,1)S(1)} all-gather(bf16[16,1024]{1,0:T(8,128)(2,1)S(1)} %multiply_convert_fusion), channel_id=1, replica_groups=mesh['ep'=16,'tp'=2] {'ep'}, dimensions={0}, use_global_device_ids=true | all-gather | bytes 557056 | tf_op jit(solution)/shard_map/all_gather | solution.py:168
  74.4 0.3 fusion.60
  74.7 1.5 %fusion.27 = f32[256,512]{1,0:T(8,128)} fusion(bf16[176,512]{1,0:T(8,128)(2,1)S(1)} %copy-done.13, bf16[256,1024]{1,0:T(8,128)(2,1)S(1)} %all_gather.11, bf16[176,1024]{1,0:T(8,128)(2,1)S(1)} %copy-done.12, f32[256,176]{0,1:T(8,128)S(1)} %fusion.60), kind=kOutput, calls=%fused_computation.23 | convolution fusion | flops 138682368 | bytes 1769472 | tf_op jit(solution)/shard_map/dot_general | solution.py:177
  76.2 3.5 %all-to-all-start.1 = ((bf16[16,16,512]{2,1,0:T(8,128)(2,1)}), bf16[16,16,512]{2,1,0:T(8,128)(2,1)S(1)}, u32[]{:S(2)}, u32[]{:S(2)}) async-start(bf16[16,16,512]{2,1,0:T(8,128)(2,1)} %reduce-scatter.3.cloned.1.call-done), calls=%async_computation.2 | async-start | bytes 524288 | tf_op jit(solution)/shard_map/all_to_all | solution.py:155
  80.0 9.7 %all-to-all-done.1 = bf16[16,16,512]{2,1,0:T(8,128)(2,1)S(1)} async-done(((bf16[16,16,512]{2,1,0:T(8,128)(2,1)}), bf16[16,16,512]{2,1,0:T(8,128)(2,1)S(1)}, u32[]{:S(2)}, u32[]{:S(2)}) %all-to-all-start.1) | async-done | bytes 262176 | tf_op jit(solution)/shard_map/all_to_all | solution.py:155
  89.8 40.1 %reduce-scatter.5.cloned.1.call-done = f32[16,512]{1,0:T(8,128)} async-done(((f32[256,512]{1,0:T(8,128)}), f32[16,512]{1,0:T(8,128)}) %reduce-scatter.5.cloned.1.call-update) | async-done | bytes 32784 | tf_op jit(solution)/shard_map/reduce_scatter | solution.py:176
  129.9 1.1 fusion.55
  130.9 4.9 %all-reduce = (f32[16]{0:T(128)S(1)}, f32[16]{0:T(128)S(1)}) all-reduce(f32[16]{0:T(128)S(1)} %get-tuple-element.6, f32[16]{0:T(128)S(1)} %get-tuple-element.5), channel_id=1, replica_groups=mesh['ep'=16,'tp'=2] {'tp'}, use_global_device_ids=true, to_apply=%region_17.18 | all-reduce | flops 32 | bytes 256 | tf_op jit(solution)/shard_map/psum | solution.py:187
  135.9 0.7 multiply_convert_fusion.1
  (67 shorter events, 2.3 us)
Async XLA Ops:
  6.5 45.1 %copy-start = (bf16[1,704,1024]{2,1,0:T(8,128)(2,1)S(1)}, bf16[1,704,1024]{2,1,0:T(8,128)(2,1)}, u32[]{:S(2)}) copy-start(bf16[1,704,1024]{2,1,0:T(8,128)(2,1)} %param.40) | copy-start | bytes 4325380
  6.5 69.7 %reduce-scatter.3.cloned.1.call-start = ((), (), s32[]{:S(2)}) async-start(), calls=%async_computation.4 | async-start | bytes 786432 | tf_op jit(solution)/shard_map/reduce_scatter | solution.py:152
  14.1 3.6 %copy-start.1 = (f32[16,8,64,64]{3,2,1,0:T(8,128)S(1)}, f32[16,8,64,64]{3,2,1,0:T(8,128)}, u32[]{:S(2)}) copy-start(f32[16,8,64,64]{3,2,1,0:T(8,128)} %param.25) | copy-start | bytes 6291460
  17.7 3.5 %copy-start.7 = (f32[512]{0:T(512)S(1)}, f32[512]{0:T(512)}, u32[]{:S(2)}) copy-start(f32[512]{0:T(512)} %param.36) | copy-start | bytes 6148
  17.7 10.8 %copy-start.2 = (bf16[16,1024]{1,0:T(8,128)(2,1)S(1)}, bf16[16,1024]{1,0:T(8,128)(2,1)}, u32[]{:S(2)}) copy-start(bf16[16,1024]{1,0:T(8,128)(2,1)} %param.24) | copy-start | bytes 98308
  17.8 11.2 %copy-start.5 = (s32[16,2]{0,1:T(2,128)S(1)}, s32[16,2]{0,1:T(2,128)}, u32[]{:S(2)}) copy-start(s32[16,2]{0,1:T(2,128)} %param.46) | copy-start | bytes 388
  17.8 11.5 %copy-start.6 = (f32[1024]{0:T(1024)S(1)}, f32[1024]{0:T(1024)}, u32[]{:S(2)}) copy-start(f32[1024]{0:T(1024)} %param.37) | copy-start | bytes 12292
  17.8 32.4 %copy-start.3 = (bf16[1,1024,704]{1,2,0:T(8,128)(2,1)S(1)}, bf16[1,1024,704]{1,2,0:T(8,128)(2,1)}, u32[]{:S(2)}) copy-start(bf16[1,1024,704]{1,2,0:T(8,128)(2,1)} %param.38) | copy-start | bytes 4325380
  29.2 21.6 %copy-start.11 = (bf16[1,1024,704]{1,2,0:T(8,128)(2,1)S(1)}, bf16[1,1024,704]{1,2,0:T(8,128)(2,1)}, u32[]{:S(2)}) copy-start(bf16[1,1024,704]{1,2,0:T(8,128)(2,1)} %param.39) | copy-start | bytes 4325380
  50.8 23.6 %copy-start.4 = (bf16[176,1024]{1,0:T(8,128)(2,1)S(1)}, bf16[176,1024]{1,0:T(8,128)(2,1)}, u32[]{:S(2)}) copy-start(bf16[176,1024]{1,0:T(8,128)(2,1)} %param.41) | copy-start | bytes 1081348
  50.8 23.9 %copy-start.12 = (bf16[176,1024]{1,0:T(8,128)(2,1)S(1)}, bf16[176,1024]{1,0:T(8,128)(2,1)}, u32[]{:S(2)}) copy-start(bf16[176,1024]{1,0:T(8,128)(2,1)} %param.42) | copy-start | bytes 1081348
  50.8 23.9 %copy-start.13 = (bf16[176,512]{1,0:T(8,128)(2,1)S(1)}, bf16[176,512]{1,0:T(8,128)(2,1)}, u32[]{:S(2)}) copy-start(bf16[176,512]{1,0:T(8,128)(2,1)} %param.43) | copy-start | bytes 540676
  51.4 28.4 %copy-start.8 = (bf16[1024]{0:T(1024)(128)(2,1)S(1)}, bf16[1024]{0:T(1024)(128)(2,1)}, u32[]{:S(2)}) copy-start(bf16[1024]{0:T(1024)(128)(2,1)} %param.44) | copy-start | bytes 6148
  51.4 28.4 %copy-start.10 = (f32[16,2]{0,1:T(2,128)S(1)}, f32[16,2]{0,1:T(2,128)}, u32[]{:S(2)}) copy-start(f32[16,2]{0,1:T(2,128)} %param.47) | copy-start | bytes 388
  51.6 84.3 %copy-start.9 = (f32[512]{0:T(512)S(1)}, f32[512]{0:T(512)}, u32[]{:S(2)}) copy-start(f32[512]{0:T(512)} %param.45) | copy-start | bytes 6148
  53.0 76.9 %reduce-scatter.5.cloned.1.call-start = ((), (), s32[]{:S(2)}) async-start(), calls=%async_computation.5 | async-start | bytes 557056 | tf_op jit(solution)/shard_map/reduce_scatter | solution.py:176
  76.2 13.5 %all-to-all-start.1 = ((bf16[16,16,512]{2,1,0:T(8,128)(2,1)}), bf16[16,16,512]{2,1,0:T(8,128)(2,1)S(1)}, u32[]{:S(2)}, u32[]{:S(2)}) async-start(bf16[16,16,512]{2,1,0:T(8,128)(2,1)} %reduce-scatter.3.cloned.1.call-done), calls=%async_computation.2 | async-start | bytes 524288 | tf_op jit(solution)/shard_map/all_to_all | solution.py:155
Sparse Core Ops, SparseCore 0:
  53.1 14.1 reduce-scatter.2
  76.3 53.4 reduce-scatter.4
